TPU v7x, 32 devices: a whole 2x2x4 slice. The times are simulated.
32 devices in a mesh: ep: 8 (over z, y), tp: 4 (over x, core).
Axes of the slice: x: 2, y: 2, z: 4, core: 2. Of those that a mesh axis runs over, the one named last changes fastest.
Arguments:
- tokens_first: bfloat16 [4096, 2048], P('ep'), may hold values from -6 to 6
- norm_gain_first: float32 [2048], replicated, may hold values from 0.1 to 1.9
- w_query: bfloat16 [2048, 512], P(None, 'tp'), may hold values from -0.125 to 0.125
- w_key: bfloat16 [2048, 512], P(None, 'tp'), may hold values from -0.125 to 0.125
- w_value: bfloat16 [2048, 1024], P(None, 'tp'), may hold values from -0.125 to 0.125
- w_outgate: bfloat16 [2048, 1024], P(None, 'tp'), may hold values from -0.125 to 0.125
- w_decay: bfloat16 [2048, 512], P(None, 'tp'), may hold values from -1 to 1
- decay_bias: float32 [64, 512], P('ep', 'tp'), may hold values from -1.3 to 12.5
- head_gain: float32 [1024], P('tp'), may hold values from 0.1 to 1.9
- w_mix_out: bfloat16 [1024, 2048], P('tp'), may hold values from -0.1875 to 0.1875
- tokens_second: bfloat16 [2048, 2048], P('ep'), may hold values from -6 to 6
- norm_gain_second: float32 [2048], replicated, may hold values from 0.1 to 1.9
- routes: int32 [2048, 2], P('ep'), may hold values from 0 to 7, all different within a row; in each aligned block of 256 rows (0 to 255, 256 to 511, ...) at most 128 rows name the same one
- route_logits: float32 [2048, 2], P('ep'), may hold values from -8 to 8
- expert_gate: bfloat16 [8, 2048, 3072], P('ep', None, 'tp'), may hold values from -0.125 to 0.125
- expert_up: bfloat16 [8, 2048, 3072], P('ep', None, 'tp'), may hold values from -0.125 to 0.125
- expert_down: bfloat16 [8, 3072, 2048], P('ep', 'tp'), may hold values from -0.109375 to 0.109375
Outputs:
- mixed_first: bfloat16 [4096, 2048], P(('ep', 'tp'))
- mixed_second: bfloat16 [2048, 2048], P('ep', 'tp')
Inputs may be any that keep to these rules, and one draw needn't show every extreme that they name: In the rows of one index of ep (aligned blocks of 256 rows) no expert is named by more than 128 rows, a bound that some block reaches; the two routes of a row name different experts.
All inputs are finite; a program needn't handle non-finite values.
Results may differ from a plain program's by a relative error of at most 0.01.
Values may be sent and summed in bfloat16 or wider, within the bound.
A program may use at most 128 MiB of HBM per device.

v0:
```python
import jax
import jax.numpy as jnp
from jax import lax
from jax.sharding import PartitionSpec as P

KEY_DIM = 64
VALUE_DIM = 128
BLOCK = 64


EPS = 1e-06
TEMPER = 16.0


def entering(shard, axis, combine, identity):
    devices, place = (lax.axis_size(axis), lax.axis_index(axis))
    everything = jax.tree.map(lambda part: lax.all_gather(part, axis), shard)
    start = jax.tree.map(
        lambda part, zero: jnp.broadcast_to(jnp.asarray(zero, part.dtype), part.shape),
        shard,
        identity,
    )

    def hop(k, before):
        reached = k < place
        new = combine(before, jax.tree.map(lambda part: part[k], everything))
        return jax.tree.map(lambda a, b: jnp.where(reached, a, b), new, before)

    return lax.fori_loop(0, devices, hop, start)


def rms_rows(rows_in, gain_row):
    wide_rows = rows_in.astype(jnp.float32)
    return (
        wide_rows
        * lax.rsqrt(jnp.mean(wide_rows * wide_rows, axis=-1, keepdims=True) + EPS)
        * gain_row
    )


def block_step(entry_state, inputs):
    queries, key_rows, value_matrix_rows, log_decay = inputs
    cumul_log = jnp.cumsum(log_decay, axis=0)
    forward_decay_rows = queries * jnp.exp(cumul_log)
    behind = key_rows * jnp.exp(-cumul_log)
    scores = jnp.einsum("thk,shk->hts", forward_decay_rows, behind, precision=lax.Precision.HIGHEST)
    block_len = queries.shape[0]
    causal = jnp.arange(block_len)[:, None] >= jnp.arange(block_len)[None, :]
    scores = jnp.where(causal[None], scores, jnp.zeros_like(scores))
    within = jnp.einsum("hts,shv->thv", scores, value_matrix_rows, precision=lax.Precision.HIGHEST)
    carried_state = jnp.einsum(
        "azm,zmj->azj", forward_decay_rows, entry_state, precision=lax.Precision.HIGHEST
    )
    final_log_decay = cumul_log[-1]
    fading_factor = key_rows * jnp.exp(final_log_decay[None] - cumul_log)
    following_state = jnp.exp(final_log_decay)[:, :, None] * entry_state + jnp.einsum(
        "drx,drm->rxm", fading_factor, value_matrix_rows, precision=lax.Precision.HIGHEST
    )
    return (following_state, within + carried_state)


def head_output(attended, out_gate, head_gain):
    scaled = attended * lax.rsqrt(jnp.mean(attended * attended, axis=-1, keepdims=True) + EPS)
    return (scaled.reshape(attended.shape[0], -1) * head_gain * jax.nn.silu(out_gate)).astype(
        jnp.bfloat16
    )


def chain_join(earlier, later):
    return (earlier[0] * later[0], later[0][:, :, None] * earlier[1] + later[1])


def body(
    tokens_first,
    norm_gain_first,
    w_query,
    w_key,
    w_value,
    w_outgate,
    w_decay,
    decay_bias,
    head_gain,
    w_mix_out,
    tokens_second,
    norm_gain_second,
    routes,
    route_logits,
    expert_gate,
    expert_up,
    expert_down,
):
    ep_count = lax.axis_size("ep")
    tp_count = lax.axis_size("tp")
    normed = rms_rows(tokens_first, norm_gain_first).astype(jnp.bfloat16)
    first_rows = normed.shape[0]
    blocks = first_rows // BLOCK
    heads_here = w_query.shape[1] // KEY_DIM
    queries = (
        jnp.dot(normed, w_query, preferred_element_type=jnp.float32) * KEY_DIM ** (-0.5)
    ).astype(jnp.bfloat16)
    key_rows = jnp.dot(normed, w_key, preferred_element_type=jnp.float32).astype(jnp.bfloat16)
    value_matrix_rows = jnp.dot(normed, w_value, preferred_element_type=jnp.float32).astype(
        jnp.bfloat16
    )
    out_gate = jnp.dot(normed, w_outgate, preferred_element_type=jnp.float32)
    decay_pre = (
        jnp.dot(normed, w_decay, preferred_element_type=jnp.float32).reshape(blocks, BLOCK, -1)
        + decay_bias[:, None, :]
    )
    log_decay = (jax.nn.log_sigmoid(decay_pre) / TEMPER).reshape(blocks, BLOCK, heads_here, KEY_DIM)
    queries, key_rows, value_matrix_rows = lax.optimization_barrier(
        (queries, key_rows, value_matrix_rows)
    )
    query_wide = queries.astype(jnp.float32).reshape(blocks, BLOCK, heads_here, KEY_DIM)
    key_wide = key_rows.astype(jnp.float32).reshape(blocks, BLOCK, heads_here, KEY_DIM)
    value_wide = value_matrix_rows.astype(jnp.float32).reshape(blocks, BLOCK, heads_here, VALUE_DIM)
    start_state = jnp.zeros((heads_here, KEY_DIM, VALUE_DIM), jnp.float32)
    end_state, local_out = lax.scan(
        block_step, start_state, (query_wide, key_wide, value_wide, log_decay)
    )
    fade_total = jnp.exp(jnp.sum(log_decay, axis=(0, 1)))
    _, incoming_state = entering(
        (fade_total, end_state),
        "ep",
        chain_join,
        (jnp.ones_like(fade_total), jnp.zeros_like(end_state)),
    )
    reach_log = jnp.cumsum(log_decay.reshape(first_rows, heads_here, KEY_DIM), axis=0)
    forward_decay_full = query_wide.reshape(first_rows, heads_here, KEY_DIM) * jnp.exp(reach_log)
    carried_state = jnp.einsum(
        "azm,zmj->azj", forward_decay_full, incoming_state, precision=lax.Precision.HIGHEST
    )
    attended = local_out.reshape(first_rows, heads_here, VALUE_DIM) + carried_state
    gated_rows = head_output(attended, out_gate, head_gain)
    mixed_first = lax.psum_scatter(
        jnp.dot(gated_rows, w_mix_out, preferred_element_type=jnp.float32),
        "tp",
        scatter_dimension=0,
        tiled=True,
    ).astype(jnp.bfloat16)
    normed_second = rms_rows(tokens_second, norm_gain_second).astype(jnp.bfloat16)
    second_rows, model_width = normed_second.shape
    route_count = routes.shape[1]
    experts_all = ep_count * expert_gate.shape[0]
    slot_room = 2 * route_count * second_rows // experts_all
    flat_routes = routes.reshape(-1)
    member = (flat_routes[:, None] == jnp.arange(experts_all, dtype=jnp.int32)[None, :]).astype(
        jnp.int32
    )
    slot_index = jnp.sum((jnp.cumsum(member, axis=0) - 1) * member, axis=1)
    target = flat_routes * slot_room + slot_index
    copy_rows = jnp.repeat(normed_second, route_count, axis=0)
    buffer = (
        jnp.zeros((experts_all * slot_room, model_width), jnp.bfloat16).at[target].set(copy_rows)
    )
    buffer = buffer.reshape(experts_all, slot_room, model_width)
    share_rows = slot_room // tp_count
    own_slots = lax.dynamic_slice_in_dim(buffer, lax.axis_index("tp") * share_rows, share_rows, 1)
    arrived = lax.all_to_all(own_slots, "ep", split_axis=0, concat_axis=0, tiled=True)
    expert_arrived = lax.all_gather(arrived, "tp", axis=1, tiled=True)
    flat_rows = expert_arrived.reshape(-1, model_width)
    gate_out = jnp.dot(flat_rows, expert_gate[0], preferred_element_type=jnp.float32)
    up_out = jnp.dot(flat_rows, expert_up[0], preferred_element_type=jnp.float32)
    hidden = (jax.nn.silu(gate_out) * up_out).astype(jnp.bfloat16)
    partial_value = jnp.dot(hidden, expert_down[0], preferred_element_type=jnp.float32)
    partial_value = partial_value.reshape(
        expert_arrived.shape[0], expert_arrived.shape[1], model_width
    )
    summed = lax.psum_scatter(
        partial_value.astype(jnp.bfloat16), "tp", scatter_dimension=2, tiled=True
    )
    returned = lax.all_to_all(summed, "ep", split_axis=0, concat_axis=0, tiled=True)
    received = returned.reshape(experts_all * slot_room, -1)
    picked = (
        jnp.take(received, target, axis=0).reshape(second_rows, route_count, -1).astype(jnp.float32)
    )
    route_share = jax.nn.sigmoid(route_logits - route_logits[:, ::-1])
    mixed_second = jnp.sum(picked * route_share[:, :, None], axis=1).astype(jnp.bfloat16)
    return (mixed_first, mixed_second)


def solution(mesh):
    in_specs = (
        P("ep", None),
        P(),
        P(None, "tp"),
        P(None, "tp"),
        P(None, "tp"),
        P(None, "tp"),
        P(None, "tp"),
        P("ep", "tp"),
        P("tp"),
        P("tp", None),
        P("ep", None),
        P(),
        P("ep", None),
        P("ep", None),
        P("ep", None, "tp"),
        P("ep", None, "tp"),
        P("ep", "tp", None),
    )
    out_specs = (P(("ep", "tp"), None), P("ep", "tp"))
    return jax.shard_map(body, mesh=mesh, in_specs=in_specs, out_specs=out_specs, check_vma=False)
```

profile of v0, /device:TPU:0, one launch (start us, length us, event | category | flops | bytes accessed | tf_op | source)
XLA Modules:
  0.0 294.6 jit_solution(18226832918064300480)
XLA Ops:
  12.4 1.5 fusion.26
  13.9 2.6 broadcast_in_dim.48
  16.6 4.1 %reshape.219 = bf16[512,2048]{1,0:T(8,128)(2,1)} reshape(bf16[256,2,2048]{2,1,0:T(2,128)(2,1)} %broadcast_in_dim.48) | data formatting | bytes 4194304 | tf_op jit(solution)/shard_map/reshape | solution.py:152
  20.8 7.2 %scatter_custom_fusion = bf16[1024,2048]{1,0:T(8,128)(2,1)} fusion(s32[512]{0:T(512)S(1)} %bitcast.152, bf16[512,2048]{1,0:T(8,128)(2,1)} %reshape.219, bf16[]{:T(256)} %constant.111.clone.1), kind=kCustom, calls=%fused_computation.48 | custom fusion | bytes 4194816 | tf_op jit(solution)/shard_map/scatter | solution.py:154
  29.3 33.0 %all_to_all.10 = bf16[8,32,2048]{2,1,0:T(8,128)(2,1)} all-to-all(bf16[8,32,2048]{2,1,0:T(8,128)(2,1)S(1)} %constant_dynamic-slice_fusion.2), channel_id=1, replica_groups=mesh['ep'=8,'tp'=4] {'ep'}, dimensions={0} | all-to-all | bytes 2097152 | tf_op jit(solution)/shard_map/all_to_all | solution.py:159
  62.6 2.2 fusion.14
  71.1 2.0 reshape.206
  74.4 1.9 add.175
  76.3 2.8 fusion.36
  80.1 2.0 copy.93
  82.1 2.2 fusion.32
  84.2 11.7 %all-gather.3.cloned.1.call-done = bf16[8,128,2048]{2,1,0:T(8,128)(2,1)} async-done(((bf16[8,32,2048]{2,1,0:T(8,128)(2,1)}), bf16[8,128,2048]{2,1,0:T(8,128)(2,1)}) %all-gather.3.cloned.1.call-update) | async-done | bytes 4194320 | tf_op jit(solution)/shard_map/all_gather | solution.py:160
  95.9 6.3 %fusion.18 = f32[1024,768]{1,0:T(8,128)S(1)} fusion(bf16[1024,2048]{1,0:T(8,128)(2,1)} %bitcast.154, bf16[1,2048,768]{2,1,0:T(8,128)(2,1)} %param.36), kind=kOutput, calls=%fused_computation.38 | convolution fusion | flops 3221225472 | bytes 10485760 | tf_op jit(solution)/shard_map/dot_general | solution.py:163
  102.2 3.7 %multiply_convert_fusion = bf16[1024,768]{1,0:T(8,128)(2,1)S(1)} fusion(f32[1024,768]{1,0:T(8,128)S(1)} %fusion.18, bf16[1024,2048]{1,0:T(8,128)(2,1)S(1)} %bitcast.155, bf16[1,2048,768]{2,1,0:T(8,128)(2,1)S(1)} %copy-done.13), kind=kOutput, calls=%fused_computation.42 | convolution fusion | flops 3225944064 | bytes 12058624 | tf_op jit(solution)/shard_map/dot_general | solution.py:162
  106.0 5.0 %convolution_convert_fusion = bf16[8,128,2048]{2,1,0:T(8,128)(2,1)} fusion(bf16[8,128,768]{2,1,0:T(8,128)(2,1)S(1)} %bitcast.156, bf16[1,768,2048]{2,1,0:T(8,128)(2,1)S(1)} %copy-done), kind=kOutput, calls=%fused_computation.36 | convolution fusion | flops 3223322624 | bytes 8912896 | tf_op jit(solution)/shard_map/dot_general | solution.py:165
  111.2 35.3 %while.27 = (s32[]{:T(128)}, f32[2,64,128]{2,1,0:T(8,128)S(1)}, f32[8,64,2,128]{3,1,0,2:T(8,128)}, f32[8,64,2,64]{3,1,2,0:T(8,128)}, f32[8,64,2,64]{3,2,1,0:T(2,...) while((s32[]{:T(128)}, f32[2,64,128]{2,1,0:T(8,128)S(1)}, ...), condition=%wide.region_3.4_spmd.clone, body=%wide.region_1.3_spmd.clone.sunk | while | flops 44691456 | bytes 1191540 | solution.py:118
  146.5 1.7 copy.98
  149.0 2.0 copy.104
  153.2 1.8 copy_bitcast_fusion.5
  155.0 4.5 %reduce-window.14 = f32[64,2,4,128]{3,0,1,2:T(8,128)S(1)} reduce-window(f32[64,2,4,128]{3,0,1,2:T(8,128)} %copy_bitcast_fusion.5, f32[]{:T(128)} %constant.98.clone.1), window={size=1x1x1x128 pad=0_0x0_0x0_0x127_0}, to_apply=%region_7.8 | reduce-window | flops 8323072 | bytes 524292 | tf_op jit(solution)/shard_map/reduce-window
  161.5 20.8 %all_gather.13 = f32[8,2,64]{2,1,0:T(2,128)S(1)} all-gather(f32[1,2,64]{2,1,0:T(2,128)} %exp.64), channel_id=1, replica_groups=mesh['ep'=8,'tp'=4] {'ep'}, dimensions={0}, use_global_device_ids=true | all-gather | bytes 4608 | tf_op jit(solution)/shard_map/all_gather | solution.py:17
  182.3 33.4 %all-gather = f32[16,64,128]{2,1,0:T(8,128)} all-gather(f32[2,64,128]{2,1,0:T(8,128)S(1)} %get-tuple-element.141), channel_id=2, replica_groups=mesh['ep'=8,'tp'=4] {'ep'}, dimensions={0}, use_global_device_ids=true | all-gather | bytes 589824 | tf_op jit(solution)/shard_map/all_gather | solution.py:17
  215.7 7.8 %while.28 = (s32[]{:T(128)}, f32[2,64,128]{2,1,0:T(8,128)S(1)}, s32[]{:T(128)}, f32[8,2,64]{2,1,0:T(2,128)S(1)}, f32[8,2,64,128]{3,2,1,0:T(8,128)}, /*index=5*/s32[]{:T(128)}, s32[]{:T(128)}) while((s32[]{:T(128)}, f32[2,64,128]{2,1,0:T(8,128)S(1)}, s32[]{:T(128)}, f32[8,2,64]{2,1,0:T(2,128)S(1)}, f32[8,2,64,128]{3,2,1,0:T(8,128)}, ...), condition=%wide.region_6.7_spmd.clone, body=%wide.region_5.6_spmd.clone.sunk | while | flops 65540 | bytes 198249 | solution.py:29
  223.5 1.9 multiply_reduce_fusion.1
  226.3 2.0 copy.105
  228.3 6.6 %fusion.33 = f32[512,2048]{1,0:T(8,128)} fusion(bf16[256,2048]{1,0:T(8,128)(2,1)} %param.30, f32[512,256]{1,0:T(8,128)} %copy.105, f32[256]{0:T(256)} %param.29, bf16[512,2048]{1,0:T(8,128)(2,1)} %copy-done.1, bf16[2048,256]{1,0:T(8,128)(2,1)} %param.26), kind=kOutput, calls=%fused_computation.65 | convolution fusion | flops 1074659328 | bytes 8913920 | tf_op jit(solution)/shard_map/dot_general | solution.py:136
  235.0 4.3 %all-to-all-start.1 = ((bf16[8,128,512]{2,1,0:T(8,128)(2,1)}), bf16[8,128,512]{2,1,0:T(8,128)(2,1)}, u32[]{:S(2)}, u32[]{:S(2)}) async-start(bf16[8,128,512]{2,1,0:T(8,128)(2,1)} %reduce-scatter.5.cloned.1.call-done), calls=%async_computation.3 | async-start | bytes 2097152 | tf_op jit(solution)/shard_map/all_to_all | solution.py:172
  240.0 36.0 %reduce-scatter.3.cloned.1.call-done = f32[128,2048]{1,0:T(8,128)} async-done(((f32[512,2048]{1,0:T(8,128)}), f32[128,2048]{1,0:T(8,128)}) %reduce-scatter.3.cloned.1.call-update) | async-done | bytes 1048592 | tf_op jit(solution)/shard_map/reduce_scatter | solution.py:135
  276.1 2.1 convert_element_type.56
  278.2 4.0 %gather_fusion = bf16[512,512]{1,0:T(8,128)(2,1)} fusion(bf16[1024,512]{1,0:T(8,128)(2,1)} %bitcast.20, s32[1024]{0:T(1024)S(1)} %pad_clamp_fusion), kind=kCustom, calls=%fused_computation | custom fusion | bytes 1050624 | tf_op jit(solution)/shard_map/jit(_take)/gather | solution.py:175
  282.2 2.0 gather.7
  284.2 3.9 %multiply_reduce_fusion = bf16[256,512]{1,0:T(8,128)(2,1)} fusion(bf16[256,2,512]{2,1,0:T(2,128)(2,1)} %gather.7, pred[256,2]{1,0:T(8,128)(4,1)S(1)} %copy.109, f32[256,2]{1,0:T(8,128)S(1)} %copy.111), kind=kLoop, calls=%fused_computation.57 | loop fusion | flops 917504 | bytes 788992 | tf_op jit(solution)/shard_map/reduce_sum | solution.py:178
  (194 shorter events, 64.4 us)
Async XLA Ops:
  7.2 98.8 %copy-start = (bf16[1,768,2048]{2,1,0:T(8,128)(2,1)S(1)}, bf16[1,768,2048]{2,1,0:T(8,128)(2,1)}, u32[]{:S(2)}) copy-start(bf16[1,768,2048]{2,1,0:T(8,128)(2,1)} %param.37) | copy-start | bytes 9437188
  7.2 88.7 %all-gather.3.cloned.1.call-start = ((), (), s32[]{:S(2)}) async-start(), calls=%async_computation.5 | async-start | bytes 5242880 | tf_op jit(solution)/shard_map/all_gather | solution.py:160
  20.8 8.5 %copy-start.9 = (s32[512,1]{0,1:T(1,128)}, s32[512,1]{0,1:T(1,128)S(1)}, u32[]{:S(2)}) copy-start(s32[512,1]{0,1:T(1,128)S(1)} %compare_select_fusion.3) | copy-start | bytes 6148
  29.3 35.5 %copy-start.8 = (f32[2048]{0:T(1024)S(1)}, f32[2048]{0:T(1024)}, u32[]{:S(2)}) copy-start(f32[2048]{0:T(1024)} %param.22) | copy-start | bytes 24580
  62.3 172.7 %reduce-scatter.5.cloned.1.call-start = ((), (), s32[]{:S(2)}) async-start(), calls=%async_computation.6 | async-start | bytes 5242880 | tf_op jit(solution)/shard_map/reduce_scatter | solution.py:169
  62.6 2.3 copy-start.2
  62.6 2.8 copy-start.5
  64.8 1.3 copy-start.15
  65.4 1.5 copy-start.1
  65.4 2.0 copy-start.14
  67.4 6.9 %copy-start.4 = (bf16[512,128]{1,0:T(8,128)(2,1)}, bf16[512,128]{1,0:T(8,128)(2,1)S(1)}, u32[]{:S(2)}) copy-start(bf16[512,128]{1,0:T(8,128)(2,1)S(1)} %fusion.30) | copy-start | bytes 393220
  67.5 5.7 %copy-start.7 = (f32[8,128]{1,0:T(8,128)S(1)}, f32[8,128]{1,0:T(8,128)}, u32[]{:S(2)}) copy-start(f32[8,128]{1,0:T(8,128)} %param.28) | copy-start | bytes 12292
  79.1 23.1 %copy-start.3 = (f32[512,128]{0,1:T(8,128)}, f32[512,128]{0,1:T(8,128)S(1)}, u32[]{:S(2)}) copy-start(f32[512,128]{0,1:T(8,128)S(1)} %get-tuple-element.248) | copy-start | bytes 786436
  95.9 6.3 %copy-start.12 = (bf16[8,128,2048]{2,1,0:T(8,128)(2,1)S(1)}, bf16[8,128,2048]{2,1,0:T(8,128)(2,1)}, u32[]{:S(2)}) copy-start(bf16[8,128,2048]{2,1,0:T(8,128)(2,1)} %all-gather.3.cloned.1.call-done) | copy-start | bytes 12582916
  95.9 6.3 %copy-start.13 = (bf16[1,2048,768]{2,1,0:T(8,128)(2,1)S(1)}, bf16[1,2048,768]{2,1,0:T(8,128)(2,1)}, u32[]{:S(2)}) copy-start(bf16[1,2048,768]{2,1,0:T(8,128)(2,1)} %param.35) | copy-start | bytes 9437188
  111.0 165.1 %reduce-scatter.3.cloned.1.call-start = ((), (), s32[]{:S(2)}) async-start(), calls=%async_computation.4 | async-start | bytes 5242880 | tf_op jit(solution)/shard_map/reduce_scatter | solution.py:135
  235.0 4.6 %copy-start.6 = (s32[256,2]{0,1:T(2,128)S(1)}, s32[256,2]{0,1:T(2,128)}, u32[]{:S(2)}) copy-start(s32[256,2]{0,1:T(2,128)} %param.33) | copy-start | bytes 6148
  235.0 4.8 %copy-start.11 = (f32[256,2]{0,1:T(2,128)S(1)}, f32[256,2]{0,1:T(2,128)}, u32[]{:S(2)}) copy-start(f32[256,2]{0,1:T(2,128)} %param.34) | copy-start | bytes 6148
  235.0 5.0 %copy-start.10 = (s32[512,1]{0,1:T(1,128)S(1)}, s32[512,1]{0,1:T(1,128)}, u32[]{:S(2)}) copy-start(s32[512,1]{0,1:T(1,128)} %copy-done.9) | copy-start | bytes 6148
  235.0 43.1 %all-to-all-start.1 = ((bf16[8,128,512]{2,1,0:T(8,128)(2,1)}), bf16[8,128,512]{2,1,0:T(8,128)(2,1)}, u32[]{:S(2)}, u32[]{:S(2)}) async-start(bf16[8,128,512]{2,1,0:T(8,128)(2,1)} %reduce-scatter.5.cloned.1.call-done), calls=%async_computation.3 | async-start | bytes 2097152 | tf_op jit(solution)/shard_map/all_to_all | solution.py:172
Sparse Core Ops, SparseCore 0:
  62.4 33.4 all-gather.2
  111.1 44.3 reduce-scatter.4
  235.1 40.8 reduce-scatter.2
where the time goes:
time: 298 us; the launch traced here: 295 us
  blocking collectives  87.2 us (29%)
  local copies, waits for them, and re-layouts  59.2 us (20%)
  waiting for transfers between devices  47.8 us (16%)
  matrix products  41.6 us (14%)
  other arithmetic  39.2 us (13%)
  between operations  14.1 us (5%)
  starting transfers between devices  4.79 us (2%)
    all_gather x2, blocking collectives, entering(): everything = jax.tree.map(lambda part: lax.all_gather(part, axis), shard)  54.2 us
    reduce_scatter x1, waiting for transfers between devices, body(): lax.psum_scatter(jnp.dot(gated_rows, w_mix_out, preferred_element_type=jn...  36 us
    all_to_all x1, blocking collectives, body(): lax.all_to_all(own_slots, 'ep', split_axis=0, concat_axis=0, tiled=True)  33 us
    dynamic_slice x16, local copies, waits for them, and re-layouts, body(): lax.scan(block_step, start_state, (query_wide, key_wide, value_wide, log_...  13.7 us
    all_gather x1, waiting for transfers between devices, body(): expert_arrived = lax.all_gather(arrived, 'tp', axis=1, tiled=True)  11.7 us
    mul x8, other arithmetic, block_step(): behind = key_rows * jnp.exp(-cumul_log)  7.97 us
    select_n x8, other arithmetic, hop(): return jax.tree.map(lambda a, b: jnp.where(reached, a, b), new, before)  7.48 us
    scatter x1, local copies, waits for them, and re-layouts, body(): jnp.zeros((experts_all * slot_room, model_width), jnp.bfloat16).at[target]  7.21 us
  transfers between devices with their start and end apart: 4, of which 2 were waited for; matrix products, arithmetic and copies ran while one was open for 31% of the time, Pallas kernels for 0%

commit v1 on v0

v1 whole, which is shorter than its diff:
```python
import functools

import jax
import jax.numpy as jnp
from jax import lax
from jax.experimental import pallas as pl
from jax.experimental.pallas import tpu as pltpu
from jax.sharding import PartitionSpec as P

KEY_DIM = 64
VALUE_DIM = 128
BLOCK = 64
EPS = 1e-06
TEMPER = 16.0
CHUNKS = 4
LANES = 128

MESH = pl.DeviceIdType.MESH
F32 = jnp.float32
BF16 = jnp.bfloat16


def flip(index, mask):
    bit = 1
    while bit <= mask:
        if mask & bit:
            index = index + bit - 2 * bit * ((index // bit) % 2)
        bit *= 2
    return index


def dot(a, b):
    return jnp.dot(a, b, preferred_element_type=F32)


def dot_t(a, b, dims):
    return lax.dot_general(a, b, (dims, ((), ())), preferred_element_type=F32)


def rms_scale(wide):
    return lax.rsqrt(jnp.mean(wide * wide, axis=-1, keepdims=True) + EPS)


def kernel(
    n_ep,
    n_tp,
    tokens_first,
    gain_first,
    w_query,
    w_key,
    w_value,
    w_outgate,
    w_decay,
    decay_bias,
    head_gain,
    w_mix_out,
    tokens_second,
    gain_second,
    routes,
    routes_t,
    logits,
    e_gate,
    e_up,
    e_down,
    out_first,
    out_second,
    tf,
    wq,
    wk,
    wv,
    wg,
    wd,
    wm,
    ts,
    eg,
    eu,
    ed,
    normed,
    q_s,
    k_s,
    v_s,
    g_s,
    cum_s,
    state_s,
    st_send,
    fade_send,
    st_recv,
    fade_recv,
    inc,
    gated,
    mixp,
    mrecv1,
    msend,
    mrecv2,
    slots,
    rows,
    hid,
    part,
    recv1,
    send2,
    recv2,
    result,
    received,
    load_sem,
    disp_ss,
    disp_rs,
    xf_ss,
    xf_rs,
    cf_ss,
    cf_rs,
    st_ss,
    st_rs,
    fd_ss,
    fd_rs,
    m1_ss,
    m1_rs,
    m2_ss,
    m2_rs,
    r1_ss,
    r1_rs,
    r2_ss,
    r2_rs,
    ret_ss,
    ret_rs,
):
    e = lax.axis_index("ep")
    t = lax.axis_index("tp")
    lo = t % 2
    hi = t // 2
    near = flip(t, 1)
    far = flip(t, 2)
    cross = flip(t, 3)
    hi_other = 1 - hi

    loads = [
        pltpu.make_async_copy(src, dst, load_sem.at[i])
        for i, (src, dst) in enumerate(
            [
                (tokens_second, ts),
                (tokens_first, tf),
                (w_query, wq),
                (w_key, wk),
                (w_decay, wd),
                (w_value, wv),
                (w_outgate, wg),
                (e_gate, eg),
                (e_up, eu),
                (e_down, ed),
                (w_mix_out, wm),
            ]
        )
    ]
    for load in loads:
        load.start()

    barrier = pltpu.get_barrier_semaphore()
    for j in range(1, n_ep):
        pl.semaphore_signal(barrier, inc=1, device_id=(flip(e, j), t), device_id_type=MESH)
    for peer in (near, far):
        pl.semaphore_signal(barrier, inc=1, device_id=(e, peer), device_id_type=MESH)

    n_rows = ts.shape[0]
    n_slots, width = slots.shape
    room = n_slots // n_ep
    expert_col = lax.broadcasted_iota(jnp.int32, (LANES, n_rows), 0)
    rt = routes_t[...]
    m0 = (expert_col == rt[0:1, :]).astype(F32)
    m1 = (expert_col == rt[1:2, :]).astype(F32)
    r_i = lax.broadcasted_iota(jnp.int32, (n_rows, n_rows), 0)
    c_i = lax.broadcasted_iota(jnp.int32, (n_rows, n_rows), 1)
    before = dot((m0 + m1).astype(BF16), (r_i < c_i).astype(BF16))
    t0 = rt[0:1, :] * room + jnp.sum(m0 * before, axis=0, keepdims=True).astype(jnp.int32)
    t1 = rt[1:2, :] * room + jnp.sum(m1 * before, axis=0, keepdims=True).astype(jnp.int32)
    loads[0].wait()
    scale2 = rms_scale(ts[...].astype(F32))
    mine = pl.ds(pl.multiple_of(t * width, width), width)
    piece = (ts[:, mine].astype(F32) * scale2 * gain_second[:, mine]).astype(BF16)

    def build(i, carry):
        start = pl.multiple_of(i * 256, 256)
        slot_id = lax.broadcasted_iota(jnp.int32, (256, n_rows), 0) + start
        pick = ((slot_id == t0) | (slot_id == t1)).astype(F32).astype(BF16)
        slots[pl.ds(start, 256), :] = dot(pick, piece).astype(BF16)
        return carry

    lax.fori_loop(0, n_slots // 256, build, 0)

    def place(s):
        return pl.ds(pl.multiple_of(s * room, room), room)

    pl.semaphore_wait(barrier, n_ep + 1)

    def remote(src, dst, ss, rs, dev):
        return pltpu.make_async_remote_copy(
            src_ref=src, dst_ref=dst, send_sem=ss, recv_sem=rs, device_id=dev, device_id_type=MESH
        )

    disp = [None]
    for j in range(1, n_ep):
        s = flip(e, j)
        disp.append(
            remote(
                slots.at[place(s), :], rows.at[t, place(e), :], disp_ss.at[j], disp_rs.at[j], (s, t)
            )
        )
        disp[j].start()
    rows[t, place(e), :] = slots[place(e), :]

    xf, cf0, cf1 = [], [], []
    for j in range(n_ep):
        p = place(flip(e, j))
        xf.append(remote(rows.at[t, p, :], rows.at[t, p, :], xf_ss.at[j], xf_rs.at[j], (e, far)))
        cf0.append(
            remote(rows.at[t, p, :], rows.at[t, p, :], cf_ss.at[j, 0], cf_rs.at[j, 0], (e, near))
        )
        cf1.append(
            remote(
                rows.at[far, p, :], rows.at[far, p, :], cf_ss.at[j, 1], cf_rs.at[j, 1], (e, near)
            )
        )
    per_chunk = n_ep // CHUNKS

    def forward_own(c):
        for j in range(c * per_chunk, (c + 1) * per_chunk):
            if j > 0:
                disp[j].wait_recv()
            xf[j].start()
            cf0[j].start()

    def forward_far(c):
        for j in range(c * per_chunk, (c + 1) * per_chunk):
            xf[j].wait_recv()
            cf1[j].start()

    def arrived(c):
        for j in range(c * per_chunk, (c + 1) * per_chunk):
            cf0[j].wait_recv()
            cf1[j].wait_recv()

    xf[0].start()
    cf0[0].start()

    loads[1].wait()
    n_first = tf.shape[0]
    blocks = n_first // BLOCK

    def norm_rows(i, carry):
        at = pl.ds(pl.multiple_of(i * BLOCK, BLOCK), BLOCK)
        wide = tf[at, :].astype(F32)
        normed[at, :] = (wide * rms_scale(wide) * gain_first[...]).astype(BF16)
        return carry

    lax.fori_loop(0, blocks, norm_rows, 0)
    loads[2].wait()
    q_s[...] = (dot(normed[...], wq[...]) * KEY_DIM ** (-0.5)).astype(BF16)
    loads[3].wait()
    k_s[...] = dot(normed[...], wk[...]).astype(BF16)
    loads[4].wait()
    cum_s[...] = dot(normed[...], wd[...])
    for j in range(1, per_chunk):
        disp[j].wait_recv()
        xf[j].start()
        cf0[j].start()
    loads[5].wait()
    v_s[...] = dot(normed[...], wv[...]).astype(BF16)
    loads[6].wait()
    g_s[...] = dot(normed[...], wg[...])
    forward_own(1)
    forward_far(0)

    keys = k_s.shape[1]
    heads = keys // KEY_DIM
    tri_r = lax.broadcasted_iota(jnp.int32, (BLOCK, BLOCK), 0)
    tri_c = lax.broadcasted_iota(jnp.int32, (BLOCK, BLOCK), 1)
    causal = tri_r >= tri_c
    tri = causal.astype(F32)
    head_of = lax.broadcasted_iota(jnp.int32, (1, keys), 1) // KEY_DIM
    inc[...] = jnp.zeros_like(inc)

    def local_pass(b, total):
        at = pl.ds(pl.multiple_of(b * BLOCK, BLOCK), BLOCK)
        pre = cum_s[at, :] + decay_bias[pl.ds(b, 1), :]
        log_decay = (jnp.minimum(pre, 0.0) - jnp.log1p(jnp.exp(-jnp.abs(pre)))) / TEMPER
        cum = jnp.dot(tri, log_decay, precision=lax.Precision.HIGHEST, preferred_element_type=F32)
        cum_s[at, :] = cum
        last = cum[BLOCK - 1 : BLOCK, :]
        fading = (k_s[at, :].astype(F32) * jnp.exp(last - cum)).astype(BF16)
        full = dot_t(v_s[at, :], fading, ((0,), (0,)))
        add = full[0:VALUE_DIM]
        for h in range(1, heads):
            add = jnp.where(head_of == h, full[h * VALUE_DIM : (h + 1) * VALUE_DIM], add)
        state_s[b] = inc[...]
        inc[...] = inc[...] * jnp.exp(last) + add
        return total + last

    total = lax.fori_loop(0, blocks, local_pass, jnp.zeros((1, keys), F32))
    st_send[...] = inc[...].astype(BF16)
    fade_send[...] = jnp.broadcast_to(jnp.exp(total), fade_send.shape)

    def state_copies(k, dst):
        return (
            remote(st_send, st_recv.at[k], st_ss.at[k], st_rs.at[k], (dst, t)),
            remote(fade_send, fade_recv.at[k], fd_ss.at[k], fd_rs.at[k], (dst, t)),
        )

    for k in range(1, n_ep):

        @pl.when(e + k < n_ep)
        def _():
            for copy in state_copies(k, e + k):
                copy.start()

    chunk_rows = n_slots // CHUNKS
    hidden_width = hid.shape[1]
    tile = 256

    def chunk_at(c):
        m = flip(e // per_chunk, c)
        return pl.ds(pl.multiple_of(m * chunk_rows, chunk_rows), chunk_rows)

    def experts(c):
        at = chunk_at(c)

        def up(i, carry):
            cols = pl.ds(pl.multiple_of(i * tile, tile), tile)
            gate = jnp.zeros((chunk_rows, tile), F32)
            upper = jnp.zeros((chunk_rows, tile), F32)
            for b in range(n_tp):
                x = rows[b, at, :]
                gate = gate + dot(x, eg[0, b * width : (b + 1) * width, cols])
                upper = upper + dot(x, eu[0, b * width : (b + 1) * width, cols])
            hid[:, cols] = (gate * jax.nn.sigmoid(gate) * upper).astype(BF16)
            return carry

        lax.fori_loop(0, hidden_width // tile, up, 0)

        def down(b, carry):
            cols = pl.ds(pl.multiple_of(b * width, width), width)
            part[b, at, :] = dot(hid[...], ed[0, :, cols]).astype(BF16)
            return carry

        lax.fori_loop(0, n_tp, down, 0)

    near_lo = 1 - lo
    r1, r2, ret = [], [], []
    for c in range(CHUNKS):
        at = chunk_at(c)
        r1.append(
            [
                remote(
                    part.at[2 * h + near_lo, at, :],
                    recv1.at[h, at, :],
                    r1_ss.at[c, h],
                    r1_rs.at[c, h],
                    (e, near),
                )
                for h in range(2)
            ]
        )
        r2.append(remote(send2.at[at, :], recv2.at[at, :], r2_ss.at[c], r2_rs.at[c], (e, far)))
    for j in range(n_ep):
        s = flip(e, j)
        ret.append(
            remote(
                result.at[place(s), :], received.at[place(e), :], ret_ss.at[j], ret_rs.at[j], (s, t)
            )
        )

    def send_near(c):
        for copy in r1[c]:
            copy.start()

    def send_far(c):
        at = chunk_at(c)
        for copy in r1[c]:
            copy.wait_recv()
        send2[at, :] = (
            part[2 * hi_other + lo, at, :].astype(F32) + recv1[hi_other, at, :].astype(F32)
        ).astype(BF16)
        r2[c].start()

    def send_back(c):
        at = chunk_at(c)
        r2[c].wait_recv()
        result[at, :] = (
            part[t, at, :].astype(F32)
            + recv1[hi, at, :].astype(F32)
            + recv2[at, :].astype(F32)
        ).astype(BF16)
        for j in range(c * per_chunk, (c + 1) * per_chunk):
            if j > 0:
                ret[j].start()
        if c == 0:
            received[place(e), :] = result[place(e), :]

    forward_own(2)
    forward_far(1)
    for load in loads[7:10]:
        load.wait()
    arrived(0)
    experts(0)
    send_near(0)
    forward_own(3)
    forward_far(2)
    arrived(1)
    experts(1)
    send_near(1)
    send_far(0)
    forward_far(3)
    arrived(2)
    experts(2)
    send_near(2)
    send_far(1)
    send_back(0)
    arrived(3)
    experts(3)
    send_near(3)
    send_far(2)
    send_back(1)

    inc[...] = jnp.zeros_like(inc)
    for k in range(n_ep - 1, 0, -1):

        @pl.when(e >= k)
        def _():
            for copy in state_copies(k, e):
                copy.wait_recv()
            inc[...] = inc[...] * fade_recv[k, 0:1, :] + st_recv[k].astype(F32)

    def final_pass(b, before_log):
        at = pl.ds(pl.multiple_of(b * BLOCK, BLOCK), BLOCK)
        cum = cum_s[at, :]
        ahead = (q_s[at, :].astype(F32) * jnp.exp(cum)).astype(BF16)
        behind = (k_s[at, :].astype(F32) * jnp.exp(-cum)).astype(BF16)
        entry = (state_s[b] + inc[...] * jnp.exp(before_log)).astype(BF16)
        for h in range(heads):
            cols = slice(h * VALUE_DIM, (h + 1) * VALUE_DIM)
            own = jnp.where(head_of == h, ahead, jnp.zeros_like(ahead))
            scores = jnp.where(causal, dot_t(own, behind, ((1,), (1,))), 0.0)
            attended = dot(scores.astype(BF16), v_s[at, cols]) + dot_t(own, entry, ((1,), (1,)))
            gate = g_s[at, cols]
            gated[at, cols] = (
                attended
                * rms_scale(attended)
                * head_gain[:, cols]
                * (gate * jax.nn.sigmoid(gate))
            ).astype(BF16)
        return before_log + cum[BLOCK - 1 : BLOCK, :]

    lax.fori_loop(0, blocks, final_pass, jnp.zeros((1, keys), F32))
    loads[10].wait()
    mix_rows = n_first // n_tp

    def mix(i, carry):
        at = pl.ds(pl.multiple_of(i * mix_rows, mix_rows), mix_rows)
        mixp[i] = dot(gated[at, :], wm[...]).astype(BF16)
        return carry

    lax.fori_loop(0, n_tp, mix, 0)
    mix1 = [
        remote(
            mixp.at[2 * h + near_lo], mrecv1.at[h], m1_ss.at[h], m1_rs.at[h], (e, near)
        )
        for h in range(2)
    ]
    for copy in mix1:
        copy.start()
    send_far(3)
    send_back(2)
    for copy in mix1:
        copy.wait_recv()
    msend[...] = (
        mixp[2 * hi_other + lo].astype(F32) + mrecv1[hi_other].astype(F32)
    ).astype(BF16)
    mix2 = remote(msend, mrecv2, m2_ss.at[0], m2_rs.at[0], (e, far))
    mix2.start()
    send_back(3)
    mix2.wait_recv()
    out_first[...] = (
        mixp[t].astype(F32) + mrecv1[hi].astype(F32) + mrecv2[...].astype(F32)
    ).astype(BF16)

    col_expert = lax.broadcasted_iota(jnp.int32, (n_rows, LANES), 1)
    route = routes[...]
    n0 = (col_expert == route[:, 0:1]).astype(F32)
    n1 = (col_expert == route[:, 1:2]).astype(F32)
    ahead_of = dot((r_i > c_i).astype(BF16), (n0 + n1).astype(BF16))
    u0 = route[:, 0:1] * room + jnp.sum(n0 * ahead_of, axis=1, keepdims=True).astype(jnp.int32)
    u1 = route[:, 1:2] * room + jnp.sum(n1 * ahead_of, axis=1, keepdims=True).astype(jnp.int32)
    log0 = logits[:, 0:1]
    log1 = logits[:, 1:2]
    slot_col = lax.broadcasted_iota(jnp.int32, (n_rows, n_slots), 1)
    pick0 = (slot_col == u0).astype(F32).astype(BF16)
    pick1 = (slot_col == u1).astype(F32).astype(BF16)
    for j in range(1, n_ep):
        ret[j].wait_recv()
    out_second[...] = (
        dot(pick0, received[...]) * jax.nn.sigmoid(log0 - log1)
        + dot(pick1, received[...]) * jax.nn.sigmoid(log1 - log0)
    ).astype(BF16)

    for j in range(n_ep):
        if j > 0:
            disp[j].wait_send()
            ret[j].wait_send()
        xf[j].wait_send()
        cf0[j].wait_send()
        cf1[j].wait_send()
    for c in range(CHUNKS):
        for copy in r1[c]:
            copy.wait_send()
        r2[c].wait_send()
    for copy in mix1:
        copy.wait_send()
    mix2.wait_send()
    for k in range(1, n_ep):

        @pl.when(e + k < n_ep)
        def _():
            for copy in state_copies(k, e + k):
                copy.wait_send()


def body(
    tokens_first,
    norm_gain_first,
    w_query,
    w_key,
    w_value,
    w_outgate,
    w_decay,
    decay_bias,
    head_gain,
    w_mix_out,
    tokens_second,
    norm_gain_second,
    routes,
    route_logits,
    expert_gate,
    expert_up,
    expert_down,
):
    n_ep = lax.axis_size("ep")
    n_tp = lax.axis_size("tp")
    n_first, model = tokens_first.shape
    n_rows = tokens_second.shape[0]
    room = 2 * routes.shape[1] * n_rows // (n_ep * expert_gate.shape[0])
    n_slots = n_ep * room
    width = model // n_tp
    keys = w_query.shape[1]
    values = w_value.shape[1]
    hidden = expert_gate.shape[2]
    blocks = n_first // BLOCK
    mix_rows = n_first // n_tp
    chunk_rows = n_slots // CHUNKS
    vmem = pltpu.VMEM
    dma = pltpu.SemaphoreType.DMA

    def like(x):
        return vmem(x.shape, x.dtype)

    whole = pl.BlockSpec(memory_space=pltpu.VMEM)
    away = pl.BlockSpec(memory_space=pl.ANY)
    scratch = [
        like(tokens_first),
        like(w_query),
        like(w_key),
        like(w_value),
        like(w_outgate),
        like(w_decay),
        like(w_mix_out),
        like(tokens_second),
        like(expert_gate),
        like(expert_up),
        like(expert_down),
        vmem((n_first, model), BF16),
        vmem((n_first, keys), BF16),
        vmem((n_first, keys), BF16),
        vmem((n_first, values), BF16),
        vmem((n_first, values), F32),
        vmem((n_first, keys), F32),
        vmem((blocks, VALUE_DIM, keys), F32),
        vmem((VALUE_DIM, keys), BF16),
        vmem((8, keys), F32),
        vmem((n_ep, VALUE_DIM, keys), BF16),
        vmem((n_ep, 8, keys), F32),
        vmem((VALUE_DIM, keys), F32),
        vmem((n_first, values), BF16),
        vmem((n_tp, mix_rows, model), BF16),
        vmem((2, mix_rows, model), BF16),
        vmem((mix_rows, model), BF16),
        vmem((mix_rows, model), BF16),
        vmem((n_slots, width), BF16),
        vmem((n_tp, n_slots, width), BF16),
        vmem((chunk_rows, hidden), BF16),
        vmem((n_tp, n_slots, width), BF16),
        vmem((2, n_slots, width), BF16),
        vmem((n_slots, width), BF16),
        vmem((n_slots, width), BF16),
        vmem((n_slots, width), BF16),
        vmem((n_slots, width), BF16),
        dma((11,)),
        dma((n_ep,)),
        dma((n_ep,)),
        dma((n_ep,)),
        dma((n_ep,)),
        dma((n_ep, 2)),
        dma((n_ep, 2)),
        dma((n_ep,)),
        dma((n_ep,)),
        dma((n_ep,)),
        dma((n_ep,)),
        dma((2,)),
        dma((2,)),
        dma((1,)),
        dma((1,)),
        dma((CHUNKS, 2)),
        dma((CHUNKS, 2)),
        dma((CHUNKS,)),
        dma((CHUNKS,)),
        dma((n_ep,)),
        dma((n_ep,)),
    ]
    return pl.pallas_call(
        functools.partial(kernel, n_ep, n_tp),
        out_shape=(
            jax.ShapeDtypeStruct((mix_rows, model), BF16),
            jax.ShapeDtypeStruct((n_rows, width), BF16),
        ),
        in_specs=[away, whole, away, away, away, away, away, whole, whole, away]
        + [away, whole, whole, whole, whole, away, away, away],
        out_specs=(whole, whole),
        scratch_shapes=scratch,
        compiler_params=pltpu.CompilerParams(
            collective_id=0, has_side_effects=True, vmem_limit_bytes=60 * 1024 * 1024
        ),
    )(
        tokens_first,
        norm_gain_first[None, :],
        w_query,
        w_key,
        w_value,
        w_outgate,
        w_decay,
        decay_bias,
        head_gain[None, :],
        w_mix_out,
        tokens_second,
        norm_gain_second[None, :],
        routes,
        routes.T,
        route_logits,
        expert_gate,
        expert_up,
        expert_down,
    )


def solution(mesh):
    in_specs = (
        P("ep", None),
        P(),
        P(None, "tp"),
        P(None, "tp"),
        P(None, "tp"),
        P(None, "tp"),
        P(None, "tp"),
        P("ep", "tp"),
        P("tp"),
        P("tp", None),
        P("ep", None),
        P(),
        P("ep", None),
        P("ep", None),
        P("ep", None, "tp"),
        P("ep", None, "tp"),
        P("ep", "tp", None),
    )
    out_specs = (P(("ep", "tp"), None), P("ep", "tp"))
    return jax.shard_map(body, mesh=mesh, in_specs=in_specs, out_specs=out_specs, check_vma=False)
```

time: 298 us -> 86.1 us (0.29)
  the two profiles are of different devices: /device:TPU:0 before, /device:TPU:8 now
where the time goes in v1:
time: 86.1 us; the launch traced here: 85.9 us
  Pallas kernels  78.7 us (91%)
  local copies, waits for them, and re-layouts  6.5 us (8%)
    pallas_call x1, Pallas kernels, body(): pl.pallas_call(functools.partial(kernel, n_ep, n_tp), out_shape=(jax.Shap...  78.7 us
    unnamed x4, local copies, waits for them, and re-layouts  6.5 us

profile of v1, /device:TPU:8, one launch (start us, length us, event | category | flops | bytes accessed | tf_op | source)
XLA Modules:
  0.0 85.9 jit_solution(5395233321874005435)
XLA Ops:
  0.6 1.5 %copy.20.logits = f32[256,2]{1,0:T(8,128)} copy(f32[256,2]{0,1:T(2,128)} %param.30) | data formatting | bytes 4096 | tf_op args[13]
  2.1 1.5 %copy.19.routes = s32[256,2]{1,0:T(8,128)} copy(s32[256,2]{0,1:T(2,128)} %param.29) | data formatting | bytes 4096 | tf_op args[12]
  3.6 78.7 %shard_map.176 = (bf16[128,2048]{1,0:T(8,128)(2,1)}, bf16[256,512]{1,0:T(8,128)(2,1)}) custom-call(bf16[512,2048]{1,0:T(8,128)(2,1)} %tokens_first.1, f32[1,2048]{1,0:T(1,128)} %bitcast.4, bf16[2048,128]{1,0:T(8,128)(2,1)} %w_query.1, bf16[2048,128]{1,0:T(8,128)(2,1)} %w_key.1, bf16[2048,256]{1,0:T(8,128)(2,1)} %w_value.1, bf16[2048,256]{1,0:T(8,128)(2,1)} %w_outgate.1, ...), custom_call_target="tpu_custom_call" | custom-call | tf_op jit(solution)/shard_map/pallas_call | solution.py:624
  82.3 1.9 %copy.23 = bf16[128,2048]{1,0:T(8,128)(2,1)} copy(bf16[128,2048]{1,0:T(8,128)(2,1)} %get-tuple-element.4) | data formatting | bytes 1048576
  84.2 1.7 %copy.24 = bf16[256,512]{1,0:T(8,128)(2,1)} copy(bf16[256,512]{1,0:T(8,128)(2,1)} %get-tuple-element.5) | data formatting | bytes 524288

commit v2 on v1

--- a/solution.py
+++ b/solution.py
@@ -56,9 +56,8 @@
     w_mix_out,
     tokens_second,
     gain_second,
-    routes,
     routes_t,
-    logits,
+    logits_t,
     e_gate,
     e_up,
     e_down,
@@ -101,9 +100,12 @@
     recv2,
     result,
     received,
+    picks,
     load_sem,
     disp_ss,
     disp_rs,
+    dup_ss,
+    dup_rs,
     xf_ss,
     xf_rs,
     cf_ss,
@@ -160,7 +162,7 @@
         pl.semaphore_signal(barrier, inc=1, device_id=(e, peer), device_id_type=MESH)
 
     n_rows = ts.shape[0]
-    n_slots, width = slots.shape
+    _, n_slots, width = slots.shape
     room = n_slots // n_ep
     expert_col = lax.broadcasted_iota(jnp.int32, (LANES, n_rows), 0)
     rt = routes_t[...]
@@ -173,14 +175,22 @@
     t1 = rt[1:2, :] * room + jnp.sum(m1 * before, axis=0, keepdims=True).astype(jnp.int32)
     loads[0].wait()
     scale2 = rms_scale(ts[...].astype(F32))
-    mine = pl.ds(pl.multiple_of(t * width, width), width)
-    piece = (ts[:, mine].astype(F32) * scale2 * gain_second[:, mine]).astype(BF16)
+
+    def features(block):
+        cols = pl.ds(pl.multiple_of(block * width, width), width)
+        return (ts[:, cols].astype(F32) * scale2 * gain_second[:, cols]).astype(BF16)
+
+    def chosen(start, count):
+        slot_id = lax.broadcasted_iota(jnp.int32, (count, n_rows), 0) + start
+        return ((slot_id == t0) | (slot_id == t1)).astype(F32).astype(BF16)
+
+    pieces = (features(t), features(far))
 
     def build(i, carry):
         start = pl.multiple_of(i * 256, 256)
-        slot_id = lax.broadcasted_iota(jnp.int32, (256, n_rows), 0) + start
-        pick = ((slot_id == t0) | (slot_id == t1)).astype(F32).astype(BF16)
-        slots[pl.ds(start, 256), :] = dot(pick, piece).astype(BF16)
+        pick = chosen(start, 256)
+        for which in range(2):
+            slots[which, pl.ds(start, 256), :] = dot(pick, pieces[which]).astype(BF16)
         return carry
 
     lax.fori_loop(0, n_slots // 256, build, 0)
@@ -195,50 +205,96 @@
             src_ref=src, dst_ref=dst, send_sem=ss, recv_sem=rs, device_id=dev, device_id_type=MESH
         )
 
-    disp = [None]
+    per_chunk = n_ep // CHUNKS
+
+    def members(c):
+        return list(range(c * per_chunk, (c + 1) * per_chunk))
+
+    doubled = 2 * per_chunk
+    disp, dup = [None], [None]
     for j in range(1, n_ep):
         s = flip(e, j)
         disp.append(
             remote(
-                slots.at[place(s), :], rows.at[t, place(e), :], disp_ss.at[j], disp_rs.at[j], (s, t)
+                slots.at[0, place(s), :],
+                rows.at[t, place(e), :],
+                disp_ss.at[j],
+                disp_rs.at[j],
+                (s, t),
             )
         )
+        if j < doubled:
+            dup.append(
+                remote(
+                    slots.at[1, place(s), :],
+                    rows.at[far, place(e), :],
+                    dup_ss.at[j],
+                    dup_rs.at[j],
+                    (s, t),
+                )
+            )
+
+    def dispatch(j):
         disp[j].start()
-    rows[t, place(e), :] = slots[place(e), :]
+        if j < doubled:
+            dup[j].start()
+
+    half_chunk = per_chunk // 2
+    early = members(0)[1:] + members(2) + members(3)[:half_chunk]
+    late = members(3)[half_chunk:] + members(1)
+    for j in early:
+        dispatch(j)
+    own_pick = chosen(e * room, room)
+    rows[t, place(e), :] = slots[0, place(e), :]
+    rows[far, place(e), :] = slots[1, place(e), :]
+    rows[near, place(e), :] = dot(own_pick, features(near)).astype(BF16)
+    rows[cross, place(e), :] = dot(own_pick, features(cross)).astype(BF16)
 
     xf, cf0, cf1 = [], [], []
     for j in range(n_ep):
         p = place(flip(e, j))
-        xf.append(remote(rows.at[t, p, :], rows.at[t, p, :], xf_ss.at[j], xf_rs.at[j], (e, far)))
+        xf.append(
+            None
+            if j < doubled
+            else remote(rows.at[t, p, :], rows.at[t, p, :], xf_ss.at[j], xf_rs.at[j], (e, far))
+        )
         cf0.append(
-            remote(rows.at[t, p, :], rows.at[t, p, :], cf_ss.at[j, 0], cf_rs.at[j, 0], (e, near))
+            None
+            if j == 0
+            else remote(
+                rows.at[t, p, :], rows.at[t, p, :], cf_ss.at[j, 0], cf_rs.at[j, 0], (e, near)
+            )
         )
         cf1.append(
-            remote(
+            None
+            if j == 0
+            else remote(
                 rows.at[far, p, :], rows.at[far, p, :], cf_ss.at[j, 1], cf_rs.at[j, 1], (e, near)
             )
         )
-    per_chunk = n_ep // CHUNKS
-
-    def forward_own(c):
-        for j in range(c * per_chunk, (c + 1) * per_chunk):
+
+    def forward_own(js):
+        for j in js:
             if j > 0:
                 disp[j].wait_recv()
-            xf[j].start()
-            cf0[j].start()
-
-    def forward_far(c):
-        for j in range(c * per_chunk, (c + 1) * per_chunk):
-            xf[j].wait_recv()
-            cf1[j].start()
+                if j >= doubled:
+                    xf[j].start()
+                cf0[j].start()
+
+    def forward_far(js):
+        for j in js:
+            if j > 0:
+                if j < doubled:
+                    dup[j].wait_recv()
+                else:
+                    xf[j].wait_recv()
+                cf1[j].start()
 
     def arrived(c):
-        for j in range(c * per_chunk, (c + 1) * per_chunk):
-            cf0[j].wait_recv()
-            cf1[j].wait_recv()
-
-    xf[0].start()
-    cf0[0].start()
+        for j in members(c):
+            if j > 0:
+                cf0[j].wait_recv()
+                cf1[j].wait_recv()
 
     loads[1].wait()
     n_first = tf.shape[0]
@@ -257,16 +313,10 @@
     k_s[...] = dot(normed[...], wk[...]).astype(BF16)
     loads[4].wait()
     cum_s[...] = dot(normed[...], wd[...])
-    for j in range(1, per_chunk):
-        disp[j].wait_recv()
-        xf[j].start()
-        cf0[j].start()
     loads[5].wait()
     v_s[...] = dot(normed[...], wv[...]).astype(BF16)
     loads[6].wait()
     g_s[...] = dot(normed[...], wg[...])
-    forward_own(1)
-    forward_far(0)
 
     keys = k_s.shape[1]
     heads = keys // KEY_DIM
@@ -310,6 +360,9 @@
             for copy in state_copies(k, e + k):
                 copy.start()
 
+    for j in late:
+        dispatch(j)
+
     chunk_rows = n_slots // CHUNKS
     hidden_width = hid.shape[1]
     tile = 256
@@ -393,30 +446,40 @@
         if c == 0:
             received[place(e), :] = result[place(e), :]
 
-    forward_own(2)
-    forward_far(1)
+    share0 = jax.nn.sigmoid(logits_t[0:1, :] - logits_t[1:2, :])
+    share1 = jax.nn.sigmoid(logits_t[1:2, :] - logits_t[0:1, :])
+    stacked = jnp.concatenate(
+        [
+            t0.astype(F32),
+            t1.astype(F32),
+            share0,
+            share1,
+            jnp.zeros((LANES - 4, n_rows), F32),
+        ],
+        axis=0,
+    )
+    columns = jnp.transpose(stacked)
+    slot_col = lax.broadcasted_iota(jnp.int32, (n_rows, n_slots), 1)
+    for which in range(2):
+        at_slot = columns[:, which : which + 1].astype(jnp.int32)
+        picks[which] = (slot_col == at_slot).astype(F32).astype(BF16)
+    weight0 = columns[:, 2:3]
+    weight1 = columns[:, 3:4]
+
+    forward_own(members(0))
+    forward_far(members(0))
+    forward_own(members(2))
     for load in loads[7:10]:
         load.wait()
     arrived(0)
     experts(0)
     send_near(0)
-    forward_own(3)
-    forward_far(2)
-    arrived(1)
-    experts(1)
-    send_near(1)
-    send_far(0)
-    forward_far(3)
+    forward_far(members(2))
     arrived(2)
+    forward_own(members(3)[:half_chunk])
     experts(2)
     send_near(2)
-    send_far(1)
-    send_back(0)
-    arrived(3)
-    experts(3)
-    send_near(3)
-    send_far(2)
-    send_back(1)
+    send_far(0)
 
     inc[...] = jnp.zeros_like(inc)
     for k in range(n_ep - 1, 0, -1):
@@ -447,7 +510,12 @@
             ).astype(BF16)
         return before_log + cum[BLOCK - 1 : BLOCK, :]
 
-    lax.fori_loop(0, blocks, final_pass, jnp.zeros((1, keys), F32))
+    before_log = lax.fori_loop(0, blocks // 2, final_pass, jnp.zeros((1, keys), F32))
+    send_far(2)
+    send_back(0)
+    lax.fori_loop(blocks // 2, blocks, final_pass, before_log)
+    forward_own(members(3)[half_chunk:])
+    forward_far(members(3))
     loads[10].wait()
     mix_rows = n_first // n_tp
 
@@ -465,8 +533,13 @@
     ]
     for copy in mix1:
         copy.start()
+    send_back(2)
+    arrived(3)
+    experts(3)
+    send_near(3)
+    forward_own(members(1))
+    forward_far(members(1))
     send_far(3)
-    send_back(2)
     for copy in mix1:
         copy.wait_recv()
     msend[...] = (
@@ -474,38 +547,34 @@
     ).astype(BF16)
     mix2 = remote(msend, mrecv2, m2_ss.at[0], m2_rs.at[0], (e, far))
     mix2.start()
+    arrived(1)
+    experts(1)
+    send_near(1)
     send_back(3)
+    send_far(1)
     mix2.wait_recv()
     out_first[...] = (
         mixp[t].astype(F32) + mrecv1[hi].astype(F32) + mrecv2[...].astype(F32)
     ).astype(BF16)
 
-    col_expert = lax.broadcasted_iota(jnp.int32, (n_rows, LANES), 1)
-    route = routes[...]
-    n0 = (col_expert == route[:, 0:1]).astype(F32)
-    n1 = (col_expert == route[:, 1:2]).astype(F32)
-    ahead_of = dot((r_i > c_i).astype(BF16), (n0 + n1).astype(BF16))
-    u0 = route[:, 0:1] * room + jnp.sum(n0 * ahead_of, axis=1, keepdims=True).astype(jnp.int32)
-    u1 = route[:, 1:2] * room + jnp.sum(n1 * ahead_of, axis=1, keepdims=True).astype(jnp.int32)
-    log0 = logits[:, 0:1]
-    log1 = logits[:, 1:2]
-    slot_col = lax.broadcasted_iota(jnp.int32, (n_rows, n_slots), 1)
-    pick0 = (slot_col == u0).astype(F32).astype(BF16)
-    pick1 = (slot_col == u1).astype(F32).astype(BF16)
+    send_back(1)
+
     for j in range(1, n_ep):
         ret[j].wait_recv()
     out_second[...] = (
-        dot(pick0, received[...]) * jax.nn.sigmoid(log0 - log1)
-        + dot(pick1, received[...]) * jax.nn.sigmoid(log1 - log0)
+        dot(picks[0], received[...]) * weight0 + dot(picks[1], received[...]) * weight1
     ).astype(BF16)
 
     for j in range(n_ep):
         if j > 0:
             disp[j].wait_send()
             ret[j].wait_send()
-        xf[j].wait_send()
-        cf0[j].wait_send()
-        cf1[j].wait_send()
+            cf0[j].wait_send()
+            cf1[j].wait_send()
+            if j < doubled:
+                dup[j].wait_send()
+            else:
+                xf[j].wait_send()
     for c in range(CHUNKS):
         for copy in r1[c]:
             copy.wait_send()
@@ -590,7 +659,7 @@
         vmem((2, mix_rows, model), BF16),
         vmem((mix_rows, model), BF16),
         vmem((mix_rows, model), BF16),
-        vmem((n_slots, width), BF16),
+        vmem((2, n_slots, width), BF16),
         vmem((n_tp, n_slots, width), BF16),
         vmem((chunk_rows, hidden), BF16),
         vmem((n_tp, n_slots, width), BF16),
@@ -599,7 +668,10 @@
         vmem((n_slots, width), BF16),
         vmem((n_slots, width), BF16),
         vmem((n_slots, width), BF16),
+        vmem((2, n_rows, n_slots), BF16),
         dma((11,)),
+        dma((n_ep,)),
+        dma((n_ep,)),
         dma((n_ep,)),
         dma((n_ep,)),
         dma((n_ep,)),
@@ -628,7 +700,7 @@
             jax.ShapeDtypeStruct((n_rows, width), BF16),
         ),
         in_specs=[away, whole, away, away, away, away, away, whole, whole, away]
-        + [away, whole, whole, whole, whole, away, away, away],
+        + [away, whole, whole, whole, away, away, away],
         out_specs=(whole, whole),
         scratch_shapes=scratch,
         compiler_params=pltpu.CompilerParams(
@@ -647,9 +719,8 @@
         w_mix_out,
         tokens_second,
         norm_gain_second[None, :],
-        routes,
         routes.T,
-        route_logits,
+        route_logits.T,
         expert_gate,
         expert_up,
         expert_down,

time: 86.1 us -> 97.7 us (1.13)
  the two profiles are of different devices: /device:TPU:8 before, /device:TPU:16 now
where the time goes in v2:
time: 97.7 us; the launch traced here: 97.5 us
  Pallas kernels  93.3 us (95%)
  local copies, waits for them, and re-layouts  3.55 us (4%)
    pallas_call x1, Pallas kernels, body(): pl.pallas_call(functools.partial(kernel, n_ep, n_tp), out_shape=(jax.Shap...  93.3 us
    unnamed x2, local copies, waits for them, and re-layouts  3.55 us

profile of v2, /device:TPU:16, one launch (start us, length us, event | category | flops | bytes accessed | tf_op | source)
XLA Modules:
  0.0 97.5 jit_solution(16940919826163947978)
XLA Ops:
  0.6 93.3 %shard_map.176 = (bf16[128,2048]{1,0:T(8,128)(2,1)}, bf16[256,512]{1,0:T(8,128)(2,1)}) custom-call(bf16[512,2048]{1,0:T(8,128)(2,1)} %tokens_first.1, f32[1,2048]{1,0:T(1,128)} %bitcast.5, bf16[2048,128]{1,0:T(8,128)(2,1)} %w_query.1, bf16[2048,128]{1,0:T(8,128)(2,1)} %w_key.1, bf16[2048,256]{1,0:T(8,128)(2,1)} %w_value.1, bf16[2048,256]{1,0:T(8,128)(2,1)} %w_outgate.1, ...), custom_call_target="tpu_custom_call" | custom-call | tf_op jit(solution)/shard_map/pallas_call | solution.py:696
  93.9 1.9 %copy.21 = bf16[128,2048]{1,0:T(8,128)(2,1)} copy(bf16[128,2048]{1,0:T(8,128)(2,1)} %get-tuple-element.4) | data formatting | bytes 1048576
  95.8 1.7 %copy.22 = bf16[256,512]{1,0:T(8,128)(2,1)} copy(bf16[256,512]{1,0:T(8,128)(2,1)} %get-tuple-element.5) | data formatting | bytes 524288

commit v3 on v2

--- a/solution.py
+++ b/solution.py
@@ -317,6 +317,8 @@
     v_s[...] = dot(normed[...], wv[...]).astype(BF16)
     loads[6].wait()
     g_s[...] = dot(normed[...], wg[...])
+    forward_own(members(0))
+    forward_far(members(0))
 
     keys = k_s.shape[1]
     heads = keys // KEY_DIM
@@ -466,20 +468,20 @@
     weight0 = columns[:, 2:3]
     weight1 = columns[:, 3:4]
 
-    forward_own(members(0))
-    forward_far(members(0))
     forward_own(members(2))
     for load in loads[7:10]:
         load.wait()
     arrived(0)
     experts(0)
     send_near(0)
+    send_far(0)
     forward_far(members(2))
     arrived(2)
-    forward_own(members(3)[:half_chunk])
     experts(2)
     send_near(2)
-    send_far(0)
+    forward_own(members(3)[:half_chunk])
+    send_far(2)
+    send_back(0)
 
     inc[...] = jnp.zeros_like(inc)
     for k in range(n_ep - 1, 0, -1):
@@ -510,12 +512,7 @@
             ).astype(BF16)
         return before_log + cum[BLOCK - 1 : BLOCK, :]
 
-    before_log = lax.fori_loop(0, blocks // 2, final_pass, jnp.zeros((1, keys), F32))
-    send_far(2)
-    send_back(0)
-    lax.fori_loop(blocks // 2, blocks, final_pass, before_log)
-    forward_own(members(3)[half_chunk:])
-    forward_far(members(3))
+    lax.fori_loop(0, blocks, final_pass, jnp.zeros((1, keys), F32))
     loads[10].wait()
     mix_rows = n_first // n_tp
 
@@ -533,31 +530,40 @@
     ]
     for copy in mix1:
         copy.start()
-    send_back(2)
-    arrived(3)
-    experts(3)
-    send_near(3)
+    forward_own(members(3)[half_chunk:])
     forward_own(members(1))
     forward_far(members(1))
-    send_far(3)
+    arrived(1)
     for copy in mix1:
         copy.wait_recv()
     msend[...] = (
         mixp[2 * hi_other + lo].astype(F32) + mrecv1[hi_other].astype(F32)
     ).astype(BF16)
-    mix2 = remote(msend, mrecv2, m2_ss.at[0], m2_rs.at[0], (e, far))
-    mix2.start()
-    arrived(1)
+    half_mix = mix_rows // 2
+    mix2 = []
+    for h in range(2):
+        at = pl.ds(h * half_mix, half_mix)
+        mix2.append(
+            remote(msend.at[at, :], mrecv2.at[at, :], m2_ss.at[h], m2_rs.at[h], (e, far))
+        )
+    mix2[0].start()
     experts(1)
     send_near(1)
+    send_back(2)
+    send_far(1)
+    forward_far(members(3))
+    arrived(3)
+    experts(3)
+    send_near(3)
+    send_back(1)
+    send_far(3)
     send_back(3)
-    send_far(1)
-    mix2.wait_recv()
+    mix2[1].start()
+    for copy in mix2:
+        copy.wait_recv()
     out_first[...] = (
         mixp[t].astype(F32) + mrecv1[hi].astype(F32) + mrecv2[...].astype(F32)
     ).astype(BF16)
-
-    send_back(1)
 
     for j in range(1, n_ep):
         ret[j].wait_recv()
@@ -581,7 +587,8 @@
         r2[c].wait_send()
     for copy in mix1:
         copy.wait_send()
-    mix2.wait_send()
+    for copy in mix2:
+        copy.wait_send()
     for k in range(1, n_ep):
 
         @pl.when(e + k < n_ep)
@@ -684,8 +691,8 @@
         dma((n_ep,)),
         dma((2,)),
         dma((2,)),
-        dma((1,)),
-        dma((1,)),
+        dma((2,)),
+        dma((2,)),
         dma((CHUNKS, 2)),
         dma((CHUNKS, 2)),
         dma((CHUNKS,)),

time: 97.7 us -> 86.9 us (0.89)
  the two profiles are of different devices: /device:TPU:16 before, /device:TPU:0 now
where the time goes in v3:
time: 86.9 us; the launch traced here: 86.7 us
  Pallas kernels  82.5 us (95%)
  local copies, waits for them, and re-layouts  3.55 us (4%)
    pallas_call x1, Pallas kernels, body(): pl.pallas_call(functools.partial(kernel, n_ep, n_tp), out_shape=(jax.Shap...  82.5 us
    unnamed x2, local copies, waits for them, and re-layouts  3.55 us

profile of v3, /device:TPU:0, one launch (start us, length us, event | category | flops | bytes accessed | tf_op | source)
XLA Modules:
  0.0 86.7 jit_solution(7030921476474125225)
XLA Ops:
  0.6 82.5 %shard_map.176 = (bf16[128,2048]{1,0:T(8,128)(2,1)}, bf16[256,512]{1,0:T(8,128)(2,1)}) custom-call(bf16[512,2048]{1,0:T(8,128)(2,1)} %tokens_first.1, f32[1,2048]{1,0:T(1,128)} %bitcast.5, bf16[2048,128]{1,0:T(8,128)(2,1)} %w_query.1, bf16[2048,128]{1,0:T(8,128)(2,1)} %w_key.1, bf16[2048,256]{1,0:T(8,128)(2,1)} %w_value.1, bf16[2048,256]{1,0:T(8,128)(2,1)} %w_outgate.1, ...), custom_call_target="tpu_custom_call" | custom-call | tf_op jit(solution)/shard_map/pallas_call | solution.py:703
  83.2 1.9 %copy.21 = bf16[128,2048]{1,0:T(8,128)(2,1)} copy(bf16[128,2048]{1,0:T(8,128)(2,1)} %get-tuple-element.4) | data formatting | bytes 1048576
  85.0 1.7 %copy.22 = bf16[256,512]{1,0:T(8,128)(2,1)} copy(bf16[256,512]{1,0:T(8,128)(2,1)} %get-tuple-element.5) | data formatting | bytes 524288
